TPU v7x, 128 devices: a whole 4x4x4 slice. The times are simulated.
128 devices in a mesh: ra: 16 (over z, x), cb: 4 (over y), dp: 2 (over core).
Axes of the slice: x: 4, y: 4, z: 4, core: 2. Of those that a mesh axis runs over, the one named last changes fastest.
Arguments:
- carried: bfloat16 [3072, 4096], P('dp', 'ra'), may hold values from -100 to 100
- branch_in: bfloat16 [3072, 4096], P('dp', 'ra'), may hold values from -12 to 12
- gain_in: float32 [4096], P('ra'), may hold values from 0.1 to 1.9
- bias_in: float32 [4096], P('ra'), may hold values from -1.8 to 1.8
- up_weight: bfloat16 [4096, 16384], P('ra', 'cb'), may hold values from -0.125 to 0.125
- down_weight: bfloat16 [16384, 4096], P('cb', 'ra'), may hold values from -0.046875 to 0.046875
- gain_out: float32 [4096], P('ra'), may hold values from 0.1 to 1.9
- bias_out: float32 [4096], P('ra'), may hold values from -1.8 to 1.8
Outputs:
- layer_out: bfloat16 [3072, 4096], P('dp', 'ra')
All inputs are finite; a program needn't handle non-finite values.
Results may differ from a plain program's by a relative error of at most 0.006.
Values may be sent and summed in bfloat16 or wider, within the bound.
A program may use at most 64 MiB of HBM per device.

v0:
```python
import jax
import jax.numpy as jnp
from jax import lax
from jax.sharding import PartitionSpec as P

residual_scale = 2.0**0.25
norm_eps = 1e-05


def copy_for_each(array, axis):
    length = lax.axis_size(axis)
    return lax.all_to_all(
        jnp.broadcast_to(array[None], (length, *array.shape)), axis, 0, 0, tiled=True
    )


def of_everyone(array, axis):
    return copy_for_each(array, axis).sum(axis=0)


def packed_total(arrays, axis):
    ravelled, at, done = (jnp.concatenate([a.reshape(-1) for a in arrays]), 0, [])
    running = of_everyone(ravelled, axis)
    for a in arrays:
        done.append(running[at : at + a.size].reshape(a.shape))
        at += a.size
    return tuple(done)


def taken_together(array, axis):
    return copy_for_each(array, axis).astype(jnp.float32).sum(axis=0)


def normalize(mixed, totals, squares, width, gain, bias):
    mean = totals[:, None] / width
    spread = squares[:, None] / width - mean * mean
    return (mixed - mean) * lax.rsqrt(spread + norm_eps) * gain + bias


def per_device(carried, branch_in, gain_in, bias_in, up_weight, down_weight, gain_out, bias_out):
    width = carried.shape[1] * lax.axis_size("ra")
    mixed_in = residual_scale * carried.astype(jnp.float32) + branch_in.astype(jnp.float32)
    totals, squares = packed_total(
        (jnp.sum(mixed_in, axis=1), jnp.sum(mixed_in * mixed_in, axis=1)), "ra"
    )
    normed = normalize(mixed_in, totals, squares, width, gain_in, bias_in).astype(jnp.bfloat16)
    regrouped = lax.all_to_all(up_weight, "ra", split_axis=1, concat_axis=0, tiled=True)
    pre_share = lax.dot_general(
        regrouped,
        lax.all_gather(normed, "ra", axis=1, tiled=True),
        (((0,), (1,)), ((), ())),
        preferred_element_type=jnp.float32,
    )
    hidden_share = jnp.square(jnp.maximum(pre_share, 0.0)).astype(jnp.bfloat16)
    branch_part = lax.dot_general(
        lax.all_gather(hidden_share, "ra", axis=0, tiled=True),
        down_weight,
        (((0,), (0,)), ((), ())),
        preferred_element_type=jnp.float32,
    )
    branch_out = taken_together(branch_part.astype(jnp.bfloat16), "cb").astype(jnp.float32)
    mixed_out = residual_scale * normed.astype(jnp.float32) + branch_out
    totals_out, squares_out = packed_total(
        (jnp.sum(mixed_out, axis=1), jnp.sum(mixed_out * mixed_out, axis=1)), "ra"
    )
    return normalize(mixed_out, totals_out, squares_out, width, gain_out, bias_out).astype(
        jnp.bfloat16
    )


def solution(mesh):
    in_specs = (
        P("dp", "ra"),
        P("dp", "ra"),
        P("ra"),
        P("ra"),
        P("ra", "cb"),
        P("cb", "ra"),
        P("ra"),
        P("ra"),
    )
    out_specs = P("dp", "ra")
    return jax.shard_map(
        per_device, mesh=mesh, in_specs=in_specs, out_specs=out_specs, check_vma=False
    )
```

profile of v0, /device:TPU:0, one launch (start us, length us, event | category | flops | bytes accessed | tf_op | source)
XLA Modules:
  0.0 324.9 jit_solution(11136814874928397678)
XLA Ops:
  6.5 0.0 copy-start
  6.5 0.0 copy-start.3
  6.5 0.0 copy-start.4
  6.5 0.0 copy-start.5
  6.5 0.0 all-gather.3.cloned.1.call-start
  6.6 2.1 fusion.3
  8.7 0.1 broadcast_in_dim.6
  8.8 16.1 %all_to_all.36 = f32[16,1,3072]{2,1,0:T(1,128)S(1)} all-to-all(f32[16,1,3072]{2,1,0:T(1,128)S(1)} %broadcast_in_dim.6), channel_id=1, replica_groups=mesh['ra'=16,'cb'=4,'dp'=2] {'ra'}, dimensions={0} | all-to-all | bytes 393216 | tf_op jit(solution)/shard_map/all_to_all | solution.py:12
  24.9 0.1 reduce_sum.65
  25.1 0.0 copy-done.3
  25.1 0.0 copy-done.4
  25.1 0.0 copy-done.5
  25.1 2.5 add_convert_fusion.1
  27.6 0.0 all-gather.3.cloned.1.call-update
  27.6 0.0 all-gather.5.cloned.1.call-start
  27.7 4.1 %copy.14 = bf16[256,4096]{0,1:T(8,128)(2,1)} copy(bf16[256,4096]{1,0:T(8,128)(2,1)} %param.12) | data formatting | bytes 4194304 | tf_op args[4]
  31.7 44.3 %all_to_all.37 = bf16[256,16,256]{0,2,1:T(8,128)(2,1)} all-to-all(bf16[256,16,256]{0,2,1:T(8,128)(2,1)} %bitcast.10), channel_id=1, replica_groups=mesh['ra'=16,'cb'=4,'dp'=2] {'ra'}, dimensions={1} | all-to-all | bytes 4194304 | tf_op jit(solution)/shard_map/all_to_all | solution.py:47
  76.0 3.9 %copy.15 = bf16[16,256,256]{2,1,0:T(8,128)(2,1)} copy(bf16[16,256,256]{1,2,0:T(8,128)(2,1)} %bitcast.9) | data formatting | bytes 4194304 | tf_op jit(solution)/shard_map/all_to_all | solution.py:47
  79.9 65.2 %all-gather.3.cloned.1.call-done = bf16[1536,4096]{1,0:T(8,128)(2,1)} async-done(((bf16[1536,256]{1,0:T(8,128)(2,1)}), bf16[1536,4096]{1,0:T(8,128)(2,1)}) %all-gather.3.cloned.1.call-update) | async-done | bytes 12582928 | tf_op jit(solution)/shard_map/all_gather | solution.py:50
  145.1 9.6 %fusion.2 = bf16[256,1536]{0,1:T(8,128)(2,1)} fusion(bf16[1536,4096]{1,0:T(8,128)(2,1)} %all-gather.3.cloned.1.call-done, bf16[4096,256]{1,0:T(8,128)(2,1)} %bitcast.11), kind=kOutput, calls=%fused_computation.5 | convolution fusion | flops 3222405120 | bytes 15466496 | tf_op jit(solution)/shard_map/dot_general | solution.py:48
  154.7 0.0 all-gather.5.cloned.1.call-update
  154.7 98.0 %all-gather.5.cloned.1.call-done = bf16[4096,1536]{0,1:T(8,128)(2,1)} async-done(((bf16[256,1536]{0,1:T(8,128)(2,1)}), bf16[4096,1536]{0,1:T(8,128)(2,1)}) %all-gather.5.cloned.1.call-update) | async-done | bytes 12582928 | tf_op jit(solution)/shard_map/all_gather | solution.py:56
  252.8 0.0 copy-done
  252.8 6.5 %convolution_convert_fusion = bf16[1536,256]{1,0:T(8,128)(2,1)S(1)} fusion(bf16[4096,1536]{0,1:T(8,128)(2,1)} %all-gather.5.cloned.1.call-done, bf16[4096,256]{1,0:T(8,128)(2,1)S(1)} %copy-done), kind=kOutput, calls=%fused_computation.4 | convolution fusion | flops 3221618688 | bytes 15466496 | tf_op jit(solution)/shard_map/dot_general | solution.py:55
  259.3 0.2 broadcast_in_dim.7
  259.5 40.3 %all_to_all.38 = bf16[4,1536,256]{2,1,0:T(8,128)(2,1)S(1)} all-to-all(bf16[4,1536,256]{2,1,0:T(8,128)(2,1)S(1)} %broadcast_in_dim.7), channel_id=1, replica_groups=mesh['ra'=16,'cb'=4,'dp'=2] {'cb'}, dimensions={0} | all-to-all | bytes 6291456 | tf_op jit(solution)/shard_map/all_to_all | solution.py:12
  299.8 0.0 copy-start.2
  299.8 0.5 convert_reduce_fusion
  300.2 0.0 copy-start.1
  300.2 1.1 copy-done.1
  301.4 0.0 copy-done.2
  301.4 0.0 copy-start.6
  301.4 0.0 copy-start.7
  301.4 0.5 fusion.4
  301.9 0.1 broadcast_in_dim.8
  302.0 13.1 %all_to_all.39 = f32[16,1,3072]{2,1,0:T(1,128)S(1)} all-to-all(f32[16,1,3072]{2,1,0:T(1,128)S(1)} %broadcast_in_dim.8), channel_id=1, replica_groups=mesh['ra'=16,'cb'=4,'dp'=2] {'ra'}, dimensions={0} | all-to-all | bytes 393216 | tf_op jit(solution)/shard_map/all_to_all | solution.py:12
  315.1 0.1 reduce_sum.69
  315.3 0.0 copy-done.6
  315.3 0.0 copy-done.7
  315.3 2.8 add_convert_fusion
  (4 shorter events, 0.0 us)
Async XLA Ops:
  6.5 246.2 %copy-start = (bf16[4096,256]{1,0:T(8,128)(2,1)S(1)}, bf16[4096,256]{1,0:T(8,128)(2,1)}, u32[]{:S(2)}) copy-start(bf16[4096,256]{1,0:T(8,128)(2,1)} %param.13) | copy-start | bytes 6291460
  6.5 18.5 %copy-start.3 = (bf16[1536,256]{1,0:T(8,128)(2,1)S(1)}, bf16[1536,256]{1,0:T(8,128)(2,1)}, u32[]{:S(2)}) copy-start(bf16[1536,256]{1,0:T(8,128)(2,1)} %param.9) | copy-start | bytes 2359300
  6.5 18.5 %copy-start.4 = (f32[256]{0:T(256)S(1)}, f32[256]{0:T(256)}, u32[]{:S(2)}) copy-start(f32[256]{0:T(256)} %param.11) | copy-start | bytes 3076
  6.5 18.5 %copy-start.5 = (f32[256]{0:T(256)S(1)}, f32[256]{0:T(256)}, u32[]{:S(2)}) copy-start(f32[256]{0:T(256)} %param.10) | copy-start | bytes 3076
  6.5 138.6 %all-gather.3.cloned.1.call-start = ((), (), s32[]{:S(2)}) async-start(), calls=%async_computation.4 | async-start | bytes 13369344 | tf_op jit(solution)/shard_map/all_gather | solution.py:50
  27.6 225.1 %all-gather.5.cloned.1.call-start = ((), (), s32[]{:S(2)}) async-start(), calls=%async_computation.5 | async-start | bytes 13369344 | tf_op jit(solution)/shard_map/all_gather | solution.py:56
  299.8 1.6 copy-start.2
  300.2 1.2 copy-start.1
  301.4 13.9 %copy-start.6 = (f32[256]{0:T(256)S(1)}, f32[256]{0:T(256)}, u32[]{:S(2)}) copy-start(f32[256]{0:T(256)} %param.15) | copy-start | bytes 3076
  301.4 13.9 %copy-start.7 = (f32[256]{0:T(256)S(1)}, f32[256]{0:T(256)}, u32[]{:S(2)}) copy-start(f32[256]{0:T(256)} %param.14) | copy-start | bytes 3076
Sparse Core Ops, SparseCore 0:
  27.7 117.3 all-gather.2
  154.9 97.8 all-gather.4
where the time goes:
time: 325 us
  waiting for transfers between devices  163 us (50%)
  blocking collectives  114 us (35%)
  matrix products  16.1 us (5%)
  between operations  13.5 us (4%)
  local copies, waits for them, and re-layouts  9.57 us (3%)
  other arithmetic  8.59 us (3%)
    all_gather x1, waiting for transfers between devices, per_device(): lax.all_gather(hidden_share, 'ra', axis=0, tiled=True)  98 us
    all_to_all x3, blocking collectives, copy_for_each(): lax.all_to_all(jnp.broadcast_to(array[None], (length, *array.shape)), axi...  69.5 us
    all_gather x1, waiting for transfers between devices, per_device(): lax.all_gather(normed, 'ra', axis=1, tiled=True)  65.2 us
    all_to_all x1, blocking collectives, per_device(): lax.all_to_all(up_weight, 'ra', split_axis=1, concat_axis=0, tiled=True)  44.3 us
    dot_general x1, matrix products, per_device(): lax.dot_general(regrouped, lax.all_gather(normed, 'ra', axis=1, tiled=Tru...  9.57 us
  transfers between devices with their start and end apart: 2, of which 2 were waited for; matrix products, arithmetic and copies ran while one was open for 2% of the time, Pallas kernels for 0%

commit v1 on v0

--- a/solution.py
+++ b/solution.py
@@ -52,8 +52,15 @@
         preferred_element_type=jnp.float32,
     )
     hidden_share = jnp.square(jnp.maximum(pre_share, 0.0)).astype(jnp.bfloat16)
+
+    def _deliver_pools(chunk):
+        return jnp.concatenate(
+            jax.lax.all_to_all(jnp.stack([chunk] * jax.lax.psum(1, "ra"), axis=0), "ra", 0, 0),
+            axis=0,
+        )
+
     branch_part = lax.dot_general(
-        lax.all_gather(hidden_share, "ra", axis=0, tiled=True),
+        _deliver_pools(hidden_share),
         down_weight,
         (((0,), (0,)), ((), ())),
         preferred_element_type=jnp.float32,

time: 325 us -> 378 us (1.16)
  blocking collectives: 114 us -> 260 us
  waiting for transfers between devices: 163 us -> 65.2 us
  local copies, waits for them, and re-layouts: 9.57 us -> 16.8 us
    all_to_all x0 -> x1, blocking collectives: none -> 147 us  [_deliver_pools(): jax.lax.all_to_all(jnp.stack([chunk] * jax.lax.psum(1, 'ra'), axis=0), 'r...]
    all_gather x1 -> x0, waiting for transfers between devices: 98 us -> none  [per_device(): lax.all_gather(hidden_share, 'ra', axis=0, tiled=True)]
    another operation x0 -> x1, local copies, waits for them, and re-layouts: none -> 5.78 us  [_deliver_pools(): jnp.stack([chunk] * jax.lax.psum(1, 'ra'), axis=0)]
  transfers between devices with their start and end apart: 2 -> 1, of which waited for: 2 -> 1; matrix products, arithmetic and copies ran while one was open for 2% -> 2% of each run, Pallas kernels for 0% -> 0%
where the time goes in v1:
time: 378 us; the launch traced here: 377 us
  blocking collectives  260 us (69%)
  waiting for transfers between devices  65.2 us (17%)
  local copies, waits for them, and re-layouts  16.8 us (4%)
  between operations  13.5 us (4%)
  matrix products  13.3 us (4%)
  other arithmetic  8.59 us (2%)
    all_to_all x1, blocking collectives, _deliver_pools(): jax.lax.all_to_all(jnp.stack([chunk] * jax.lax.psum(1, 'ra'), axis=0), 'r...  147 us
    all_to_all x3, blocking collectives, copy_for_each(): lax.all_to_all(jnp.broadcast_to(array[None], (length, *array.shape)), axi...  68 us
    all_gather x1, waiting for transfers between devices, per_device(): lax.all_gather(normed, 'ra', axis=1, tiled=True)  65.2 us
    all_to_all x1, blocking collectives, per_device(): lax.all_to_all(up_weight, 'ra', split_axis=1, concat_axis=0, tiled=True)  44.3 us
    dot_general x1, matrix products, per_device(): lax.dot_general(regrouped, lax.all_gather(normed, 'ra', axis=1, tiled=Tru...  9.58 us
  transfers between devices with their start and end apart: 1, of which 1 were waited for; matrix products, arithmetic and copies ran while one was open for 2% of the time, Pallas kernels for 0%

profile of v1, /device:TPU:0, one launch (start us, length us, event | category | flops | bytes accessed | tf_op | source)
XLA Modules:
  0.0 377.0 jit_solution(10895604707394252497)
XLA Ops:
  6.5 0.0 copy-start
  6.5 0.0 copy-start.3
  6.5 0.0 copy-start.4
  6.5 0.0 copy-start.5
  6.5 0.0 all-gather.2.cloned.1.call-start
  6.6 2.1 fusion.3
  8.7 0.1 broadcast_in_dim.6
  8.8 16.1 %all_to_all.41 = f32[16,1,3072]{2,1,0:T(1,128)S(1)} all-to-all(f32[16,1,3072]{2,1,0:T(1,128)S(1)} %broadcast_in_dim.6), channel_id=1, replica_groups=mesh['ra'=16,'cb'=4,'dp'=2] {'ra'}, dimensions={0} | all-to-all | bytes 393216 | tf_op jit(solution)/shard_map/all_to_all | solution.py:12
  24.9 0.1 reduce_sum.65
  25.1 0.0 copy-done.3
  25.1 0.0 copy-done.4
  25.1 0.0 copy-done.5
  25.1 2.5 add_convert_fusion.1
  27.6 0.0 all-gather.2.cloned.1.call-update
  27.6 4.1 %copy.18 = bf16[256,4096]{0,1:T(8,128)(2,1)} copy(bf16[256,4096]{1,0:T(8,128)(2,1)} %param.12) | data formatting | bytes 4194304 | tf_op args[4]
  31.7 44.3 %all_to_all.42 = bf16[256,16,256]{0,2,1:T(8,128)(2,1)} all-to-all(bf16[256,16,256]{0,2,1:T(8,128)(2,1)} %bitcast.12), channel_id=1, replica_groups=mesh['ra'=16,'cb'=4,'dp'=2] {'ra'}, dimensions={1} | all-to-all | bytes 4194304 | tf_op jit(solution)/shard_map/all_to_all | solution.py:47
  76.0 3.9 %copy.19 = bf16[16,256,256]{2,1,0:T(8,128)(2,1)} copy(bf16[16,256,256]{1,2,0:T(8,128)(2,1)} %bitcast.11) | data formatting | bytes 4194304 | tf_op jit(solution)/shard_map/all_to_all | solution.py:47
  79.9 65.2 %all-gather.2.cloned.1.call-done = bf16[1536,4096]{1,0:T(8,128)(2,1)} async-done(((bf16[1536,256]{1,0:T(8,128)(2,1)}), bf16[1536,4096]{1,0:T(8,128)(2,1)}) %all-gather.2.cloned.1.call-update) | async-done | bytes 12582928 | tf_op jit(solution)/shard_map/all_gather | solution.py:50
  145.1 9.6 %fusion.2 = bf16[256,1536]{0,1:T(8,128)(2,1)} fusion(bf16[1536,4096]{1,0:T(8,128)(2,1)} %all-gather.2.cloned.1.call-done, bf16[4096,256]{1,0:T(8,128)(2,1)} %bitcast.13), kind=kOutput, calls=%fused_computation.5 | convolution fusion | flops 3222405120 | bytes 15466496 | tf_op jit(solution)/shard_map/dot_general | solution.py:48
  154.7 1.4 copy.20
  156.1 5.8 %stack.2 = bf16[16,256,1536]{2,1,0:T(8,128)(2,1)} broadcast(bf16[256,1536]{1,0:T(8,128)(2,1)S(1)} %copy.20), dimensions={1,2} | broadcast | bytes 13369344 | tf_op jit(solution)/shard_map/stack | solution.py:58
  161.9 147.3 %all_to_all.43 = bf16[16,256,1536]{2,1,0:T(8,128)(2,1)S(1)} all-to-all(bf16[16,256,1536]{2,1,0:T(8,128)(2,1)} %stack.2), channel_id=1, replica_groups=mesh['ra'=16,'cb'=4,'dp'=2] {'ra'}, dimensions={0} | all-to-all | bytes 25165824 | tf_op jit(solution)/shard_map/all_to_all | solution.py:58
  309.2 0.0 copy-done
  309.2 3.7 convolution_convert_fusion
  312.9 0.2 broadcast_in_dim.7
  313.1 38.5 %all_to_all.44 = bf16[4,1536,256]{2,1,0:T(8,128)(2,1)S(1)} all-to-all(bf16[4,1536,256]{2,1,0:T(8,128)(2,1)S(1)} %broadcast_in_dim.7), channel_id=1, replica_groups=mesh['ra'=16,'cb'=4,'dp'=2] {'cb'}, dimensions={0} | all-to-all | bytes 6291456 | tf_op jit(solution)/shard_map/all_to_all | solution.py:12
  351.6 0.0 copy-start.2
  351.6 0.5 convert_reduce_fusion
  352.1 0.0 copy-start.1
  352.1 1.1 copy-done.1
  353.2 0.0 copy-done.2
  353.2 0.0 copy-start.6
  353.2 0.0 copy-start.7
  353.2 0.5 fusion.4
  353.8 0.1 broadcast_in_dim.8
  353.9 13.4 %all_to_all.45 = f32[16,1,3072]{2,1,0:T(1,128)S(1)} all-to-all(f32[16,1,3072]{2,1,0:T(1,128)S(1)} %broadcast_in_dim.8), channel_id=1, replica_groups=mesh['ra'=16,'cb'=4,'dp'=2] {'ra'}, dimensions={0} | all-to-all | bytes 393216 | tf_op jit(solution)/shard_map/all_to_all | solution.py:12
  367.2 0.1 reduce_sum.69
  367.4 0.0 copy-done.6
  367.4 0.0 copy-done.7
  367.4 2.8 add_convert_fusion
  (4 shorter events, 0.0 us)
Async XLA Ops:
  6.5 302.7 %copy-start = (bf16[4096,256]{1,0:T(8,128)(2,1)S(1)}, bf16[4096,256]{1,0:T(8,128)(2,1)}, u32[]{:S(2)}) copy-start(bf16[4096,256]{1,0:T(8,128)(2,1)} %param.13) | copy-start | bytes 6291460
  6.5 18.5 %copy-start.3 = (bf16[1536,256]{1,0:T(8,128)(2,1)S(1)}, bf16[1536,256]{1,0:T(8,128)(2,1)}, u32[]{:S(2)}) copy-start(bf16[1536,256]{1,0:T(8,128)(2,1)} %param.9) | copy-start | bytes 2359300
  6.5 18.5 %copy-start.4 = (f32[256]{0:T(256)S(1)}, f32[256]{0:T(256)}, u32[]{:S(2)}) copy-start(f32[256]{0:T(256)} %param.11) | copy-start | bytes 3076
  6.5 18.5 %copy-start.5 = (f32[256]{0:T(256)S(1)}, f32[256]{0:T(256)}, u32[]{:S(2)}) copy-start(f32[256]{0:T(256)} %param.10) | copy-start | bytes 3076
  6.5 138.5 %all-gather.2.cloned.1.call-start = ((), (), s32[]{:S(2)}) async-start(), calls=%async_computation.5 | async-start | bytes 13369344 | tf_op jit(solution)/shard_map/all_gather | solution.py:50
  351.6 1.6 copy-start.2
  352.1 1.2 copy-start.1
  353.2 14.2 %copy-start.6 = (f32[256]{0:T(256)S(1)}, f32[256]{0:T(256)}, u32[]{:S(2)}) copy-start(f32[256]{0:T(256)} %param.15) | copy-start | bytes 3076
  353.2 14.2 %copy-start.7 = (f32[256]{0:T(256)S(1)}, f32[256]{0:T(256)}, u32[]{:S(2)}) copy-start(f32[256]{0:T(256)} %param.14) | copy-start | bytes 3076
Sparse Core Ops, SparseCore 0:
  27.7 117.3 all-gather.1
